TPU v7x, 32 devices: a whole 2x2x4 slice. The times are simulated.
32 devices in a mesh: sp: 8 (over z, core), tp: 4 (over y, x).
Axes of the slice: x: 2, y: 2, z: 4, core: 2. Of those that a mesh axis runs over, the one named last changes fastest.
Arguments:
- residual: bfloat16 [3072, 4096], P('sp', 'tp'), may hold values from -10 to 10
- query_nope: bfloat16 [3072, 1024], P('sp', 'tp'), may hold values from -6 to 6
- query_rope: bfloat16 [3072, 512], P('sp', 'tp'), may hold values from -10 to 10
- latent: bfloat16 [3072, 512], P('sp'), may hold values from -8 to 8
- key_rope: bfloat16 [3072, 32], P('sp'), may hold values from -10 to 10
- latent_gain: float32 [512], replicated, may hold values from 0.1 to 1.9
- key_up: bfloat16 [512, 1024], P(None, 'tp'), may hold values from -0.25 to 0.25
- value_up: bfloat16 [512, 1024], P(None, 'tp'), may hold values from -0.25 to 0.25
- out_proj: bfloat16 [1024, 4096], P(None, 'tp'), may hold values from -0.625 to 0.625
- norm_gain: float32 [4096], P('tp'), may hold values from 0.1 to 1.9
- routes: int32 [3072, 2], P('sp'), may hold values from 0 to 7, all different within a row; in each aligned block of 384 rows (0 to 383, 384 to 767, ...) at most 120 rows name the same one
- route_weight: float32 [3072, 2], P('sp'), may hold values from 0.2 to 1
- expert_gate: bfloat16 [8, 4096, 1024], P('sp', None, 'tp'), may hold values from -0.09375 to 0.09375
- expert_up: bfloat16 [8, 4096, 1024], P('sp', None, 'tp'), may hold values from -0.09375 to 0.09375
- expert_down: bfloat16 [8, 1024, 4096], P('sp', None, 'tp'), may hold values from -0.1875 to 0.1875
Outputs:
- mixed_out: bfloat16 [3072, 4096], P('sp', 'tp')
Inputs may be any that keep to these rules, and one draw needn't show every extreme that they name: `routes`: each row names 2 different experts. In each aligned block of 384 rows no expert is named more than 120 times, and in some blocks one expert is named exactly 120 times.
All inputs are finite; a program needn't handle non-finite values.
Results may differ from a plain program's by a relative error of at most 0.01.
Values may be sent and summed in bfloat16 or wider, within the bound.
A program may use at most 64 MiB of HBM per device.

v0:
```python
import jax
import jax.numpy as jnp
from jax import lax
from jax.sharding import PartitionSpec as P

MODEL_DIM = 4096
NOPE_DIM = 64
ROPE_DIM = 32
VALUE_DIM = 64
TOP_K = 2


epsilon = 1e-06
rope_base = 10000.0
negative = -1e30
span_limit = 1024


def rotate(values_in, places):
    half_dim = values_in.shape[-1] // 2
    inverse = rope_base ** (-jnp.arange(half_dim, dtype=jnp.float32) / half_dim)
    angles = places.astype(jnp.float32)[:, None] * inverse[None, :]
    angles = angles.reshape((angles.shape[0],) + (1,) * (values_in.ndim - 2) + (half_dim,))
    cosine = jnp.cos(angles)
    sine_wave = jnp.sin(angles)
    first_half = values_in[..., :half_dim]
    second_half = values_in[..., half_dim:]
    return jnp.concatenate(
        [
            first_half * cosine - second_half * sine_wave,
            first_half * sine_wave + second_half * cosine,
        ],
        axis=-1,
    )


def norm_rows(values_in, gain_vec):
    wide = values_in.astype(jnp.float32)
    mean_square = jnp.mean(wide * wide, axis=-1, keepdims=True)
    return (wide * lax.rsqrt(mean_square + epsilon) * gain_vec[None, :]).astype(jnp.bfloat16)


def per_device(
    residual,
    query_nope,
    query_rope,
    latent,
    key_rope,
    latent_gain,
    key_up,
    value_up,
    out_proj,
    norm_gain,
    routes,
    route_weight,
    expert_gate,
    expert_up,
    expert_down,
):
    tok_rows = residual.shape[0]
    head_dev = query_nope.shape[1] // NOPE_DIM
    offset = lax.axis_index("sp") * tok_rows
    places = offset + jnp.arange(tok_rows, dtype=jnp.int32)
    last_row = offset + tok_rows - 1
    rot_query = rotate(
        query_rope.astype(jnp.float32).reshape(tok_rows, head_dev, ROPE_DIM), places
    ).astype(jnp.bfloat16)
    rot_key = rotate(key_rope.astype(jnp.float32), places).astype(jnp.bfloat16)
    lat_norm = norm_rows(latent, latent_gain)
    query_heads = query_nope.reshape(tok_rows, head_dev, NOPE_DIM)
    score_scale = (NOPE_DIM + ROPE_DIM) ** (-0.5)
    start_state = (
        jnp.full((tok_rows, head_dev), negative, jnp.float32),
        jnp.zeros((tok_rows, head_dev), jnp.float32),
        jnp.zeros((tok_rows, head_dev, VALUE_DIM), jnp.float32),
    )

    def update(carried, key_block, value_block, rope_block, begin_row):
        scores = (
            jnp.einsum("thd,shd->ths", query_heads, key_block, preferred_element_type=jnp.float32)
            + jnp.einsum("thr,sr->ths", rot_query, rope_block, preferred_element_type=jnp.float32)
        ) * score_scale
        key_places = begin_row + jnp.arange(key_block.shape[0], dtype=jnp.int32)
        allowed = (key_places[None, :] <= places[:, None])[:, None, :]
        scores = jnp.where(allowed, scores, negative)
        top_old, sum_old, acc_old = carried
        top_new = jnp.maximum(top_old, jnp.max(scores, axis=-1))
        weights = jnp.where(allowed, jnp.exp(scores - top_new[:, :, None]), 0.0)
        fading = jnp.exp(top_old - top_new)
        sum_new = sum_old * fading + jnp.sum(weights, axis=-1)
        acc_new = acc_old * fading[:, :, None] + jnp.einsum(
            "ths,shd->thd",
            weights.astype(jnp.bfloat16),
            value_block,
            preferred_element_type=jnp.float32,
        )
        return (top_new, sum_new, acc_new)

    def absorb(carried, key_heads, value_heads, rope_keys):
        key_count = key_heads.shape[0]
        block_len = key_count
        while block_len > span_limit and block_len % 2 == 0:
            block_len = block_len // 2
        rounds = key_count // block_len

        def stepper(carry_in, blocks):
            key_block, value_block, rope_block, begin_row = blocks
            carry_out = lax.cond(
                begin_row <= last_row,
                lambda inner: update(inner, key_block, value_block, rope_block, begin_row),
                lambda inner: inner,
                carry_in,
            )
            return (carry_out, None)

        blocks = (
            key_heads.reshape(rounds, block_len, head_dev, NOPE_DIM),
            value_heads.reshape(rounds, block_len, head_dev, VALUE_DIM),
            rope_keys.reshape(rounds, block_len, ROPE_DIM),
            block_len * jnp.arange(rounds, dtype=jnp.int32),
        )
        carried, _ = lax.scan(stepper, carried, blocks)
        return carried

    lat_piece = lax.all_gather(lat_norm, "sp", axis=0, tiled=True)
    rope_piece = lax.all_gather(rot_key, "sp", axis=0, tiled=True)
    piece_rows = lat_piece.shape[0]

    def compute_piece(inner):
        key_heads = jnp.dot(lat_piece, key_up, preferred_element_type=jnp.float32).astype(
            jnp.bfloat16
        )
        value_heads = jnp.dot(lat_piece, value_up, preferred_element_type=jnp.float32).astype(
            jnp.bfloat16
        )
        return absorb(
            inner,
            key_heads.reshape(piece_rows, head_dev, NOPE_DIM),
            value_heads.reshape(piece_rows, head_dev, VALUE_DIM),
            rope_piece,
        )

    final_state = lax.cond(
        jnp.int32(0) <= last_row, compute_piece, lambda inner: inner, start_state
    )
    attended = (
        (final_state[2] / final_state[1][:, :, None])
        .reshape(tok_rows, head_dev * VALUE_DIM)
        .astype(jnp.bfloat16)
    )
    columns = out_proj.shape[1]
    projected = jnp.dot(
        lax.all_gather(attended, "tp", axis=1, tiled=True),
        out_proj,
        preferred_element_type=jnp.float32,
    )
    mid_rows = (residual.astype(jnp.float32) + projected).astype(jnp.bfloat16)
    mid_wide = mid_rows.astype(jnp.float32)
    square = lax.psum(jnp.sum(mid_wide * mid_wide, axis=1), "tp")
    row_scale = lax.rsqrt(square / MODEL_DIM + epsilon)
    normed = (mid_wide * row_scale[:, None] * norm_gain[None, :]).astype(jnp.bfloat16)
    local_experts = expert_gate.shape[0]
    experts_all = local_experts * lax.axis_size("sp")
    capacity = 5 * tok_rows * TOP_K // (4 * experts_all)
    flat_routes = routes.reshape(-1)
    choose = (flat_routes[:, None] == jnp.arange(experts_all, dtype=jnp.int32)[None, :]).astype(
        jnp.int32
    )
    number = jnp.sum((jnp.cumsum(choose, axis=0) - 1) * choose, axis=1)
    slot_index = flat_routes * capacity + number
    source = jnp.arange(tok_rows * TOP_K, dtype=jnp.int32) // TOP_K
    slot_table = jnp.full((experts_all * capacity,), tok_rows, jnp.int32).at[slot_index].set(source)
    padded = jnp.concatenate([normed, jnp.zeros((1, columns), jnp.bfloat16)], axis=0)
    send_rows = padded[slot_table].reshape(experts_all, capacity, columns)
    arrived = lax.all_to_all(send_rows, "sp", split_axis=0, concat_axis=0, tiled=True)
    sources = arrived.shape[0] // local_experts
    item_count = arrived.shape[1]
    grouped = arrived.reshape(sources, local_experts, item_count, columns)
    grouped = jnp.swapaxes(grouped, 0, 1).reshape(local_experts, sources * item_count, columns)
    pieces = lax.all_gather(grouped, "tp", axis=2, tiled=True)
    gate_pre = jnp.einsum("erd,edf->erf", pieces, expert_gate, preferred_element_type=jnp.float32)
    up_pre = jnp.einsum("erd,edf->erf", pieces, expert_up, preferred_element_type=jnp.float32)
    hidden = (jax.nn.silu(gate_pre) * up_pre).astype(jnp.bfloat16)
    result = jnp.einsum(
        "erf,efd->erd",
        lax.all_gather(hidden, "tp", axis=2, tiled=True),
        expert_down,
        preferred_element_type=jnp.float32,
    ).astype(jnp.bfloat16)
    result = jnp.swapaxes(result.reshape(local_experts, sources, item_count, columns), 0, 1)
    result = result.reshape(sources * local_experts, item_count, columns)
    returned = lax.all_to_all(result, "sp", split_axis=0, concat_axis=0, tiled=True)
    gathered = returned.reshape(experts_all * capacity, columns)[slot_index]
    weighted = (
        gathered.astype(jnp.float32).reshape(tok_rows, TOP_K, columns) * route_weight[:, :, None]
    )
    return (mid_wide + jnp.sum(weighted, axis=1)).astype(jnp.bfloat16)


def solution(mesh):
    in_specs = (
        P("sp", "tp"),
        P("sp", "tp"),
        P("sp", "tp"),
        P("sp", None),
        P("sp", None),
        P(),
        P(None, "tp"),
        P(None, "tp"),
        P(None, "tp"),
        P("tp"),
        P("sp", None),
        P("sp", None),
        P("sp", None, "tp"),
        P("sp", None, "tp"),
        P("sp", None, "tp"),
    )
    out_specs = P("sp", "tp")
    return jax.shard_map(
        per_device, mesh=mesh, in_specs=in_specs, out_specs=out_specs, check_vma=False
    )
```

profile of v0, /device:TPU:9, one launch (start us, length us, event | category | flops | bytes accessed | tf_op | source)
XLA Modules:
  0.0 407.4 jit_solution(13175931445792578003)
XLA Ops:
  17.4 16.0 %all_gather.16 = bf16[3072,32]{0,1:T(8,128)(2,1)S(1)} all-gather(bf16[384,32]{0,1:T(8,128)(2,1)S(1)} %pad_maximum_fusion.1), channel_id=1, replica_groups=mesh['sp'=8,'tp'=4] {'sp'}, dimensions={0}, use_global_device_ids=true | all-gather | bytes 221184 | tf_op jit(solution)/shard_map/all_gather | solution.py:126
  33.5 16.7 %all-gather.5.cloned.1.call-done = bf16[3072,512]{1,0:T(8,128)(2,1)} async-done(((bf16[384,512]{1,0:T(8,128)(2,1)}), bf16[3072,512]{1,0:T(8,128)(2,1)}) %all-gather.5.cloned.1.call-update) | async-done | bytes 3145744 | tf_op jit(solution)/shard_map/all_gather | solution.py:125
  50.1 55.5 %conditional.2 = (f32[384,4]{0,1:T(4,128)}, f32[384,4,64]{0,2,1:T(8,128)}) conditional(s32[]{:T(128)} %convert_element_type.81, () %tuple.28, (bf16[3072,512]{1,0:T(8,128)(2,1)}, bf16[512,256]{1,0:T(8,128)(2,1)S(1)}, bf16[512,256]{1,0:T(8,128)(2,1)S(1)}, bf16[3072,32]{0,1:T(8,128)(2,1)S(1)}, bf16[384,256]{1,0:T(8,128)(2,1)S(1)}, /*index=5*/s32[]{:T(128)}, ...), branch_computations={%region_1.0_spmd, %region_2.9_spmd} | conditional | flops 2001965184 | bytes 50536400 | solution.py:143
  54.2 5.8 %reshape.252 = bf16[4,768,4,64]{3,2,1,0:T(4,128)(2,1)} reshape(bf16[3072,256]{1,0:T(8,128)(2,1)} %convolution_convert_fusion.1) | data formatting | bytes 3145728 | tf_op jit(solution)/shard_map/cond/branch_1_fun/reshape;cond/branch_1_fun/reshape | solution.py:117
  59.9 5.4 %copy.33 = bf16[4,768,4,64]{1,3,2,0:T(8,128)(2,1)} copy(bf16[4,768,4,64]{3,2,1,0:T(4,128)(2,1)} %reshape.252) | data formatting | bytes 3145728 | tf_op jit(solution)/shard_map/cond/branch_1_fun/while | solution.py:122
  65.4 4.1 %convolution_convert_fusion = bf16[3072,256]{1,0:T(8,128)(2,1)} fusion(bf16[3072,512]{1,0:T(8,128)(2,1)} %get-tuple-element.193, bf16[512,256]{1,0:T(8,128)(2,1)S(1)} %get-tuple-element.209), kind=kOutput, calls=%fused_computation.30 | convolution fusion | flops 806092800 | bytes 4980736 | tf_op jit(solution)/shard_map/cond/branch_1_fun/dot_general | solution.py:133
  69.5 5.8 %reshape.253 = bf16[4,768,4,64]{3,2,1,0:T(4,128)(2,1)} reshape(bf16[3072,256]{1,0:T(8,128)(2,1)} %convolution_convert_fusion) | data formatting | bytes 3145728 | tf_op jit(solution)/shard_map/cond/branch_1_fun/reshape;cond/branch_1_fun/reshape | solution.py:118
  75.2 5.4 %copy.35 = bf16[4,768,4,64]{1,3,2,0:T(8,128)(2,1)} copy(bf16[4,768,4,64]{3,2,1,0:T(4,128)(2,1)} %reshape.253) | data formatting | bytes 3145728 | tf_op jit(solution)/shard_map/cond/branch_1_fun/while | solution.py:122
  82.2 23.4 %while.13 = (s32[]{:T(128)}, f32[384,4]{0,1:T(4,128)S(1)}, f32[384,4]{0,1:T(4,128)}, f32[384,4,64]{0,2,1:T(8,128)}, s32[4]{0:T(128)S(1)}, /*index=5*/s32[]{:T(12...) while((s32[]{:T(128)}, f32[384,4]{0,1:T(4,128)S(1)}, ...), condition=%wide.region_8.8_spmd, body=%wide.region_3.7_spmd.sunk | while | flops 389779200 | bytes 26796848 | solution.py:122
  83.5 9.0 %conditional.4 = ((f32[384,4]{0,1:T(4,128)S(1)}, f32[384,4]{0,1:T(4,128)}, f32[384,4,64]{0,2,1:T(8,128)})) conditional(s32[]{:T(128)} %convert_element_type.137, (f32[384,4]{0,1:T(4,128)S(1)}, f32[384,4]{0,1:T(4,128)}, f32[384,4,64]{0,2,1:T(8,128)}) %tuple.52, (s32[]{:T(128)}, s32[384]{0:T(512)S(1)}, bf16[4,768,4,64]{1,3,2,0:T(8,128)(2,1)}, ...), branch_computations={%region_4.3_spmd, %region_5.6_spmd} | conditional | flops 389779200 | bytes 26796584 | solution.py:108
  93.9 9.0 %conditional.4 = ((f32[384,4]{0,1:T(4,128)S(1)}, f32[384,4]{0,1:T(4,128)}, f32[384,4,64]{0,2,1:T(8,128)})) conditional(s32[]{:T(128)} %convert_element_type.137, (f32[384,4]{0,1:T(4,128)S(1)}, f32[384,4]{0,1:T(4,128)}, f32[384,4,64]{0,2,1:T(8,128)}) %tuple.52, (s32[]{:T(128)}, s32[384]{0:T(512)S(1)}, bf16[4,768,4,64]{1,3,2,0:T(8,128)(2,1)}, ...), branch_computations={%region_4.3_spmd, %region_5.6_spmd} | conditional | flops 389779200 | bytes 26796584 | solution.py:108
  106.7 10.9 %all_gather.17 = bf16[384,1024]{0,1:T(8,128)(2,1)S(1)} all-gather(bf16[384,256]{0,1:T(8,128)(2,1)S(1)} %bitcast.86), channel_id=1, replica_groups=mesh['sp'=8,'tp'=4] {'tp'}, dimensions={1}, use_global_device_ids=true | all-gather | bytes 983040 | tf_op jit(solution)/shard_map/all_gather | solution.py:153
  120.5 7.2 %psum.7 = f32[384]{0:T(512)S(1)} all-reduce(f32[384]{0:T(512)S(1)} %get-tuple-element.289), channel_id=1, replica_groups=mesh['sp'=8,'tp'=4] {'tp'}, use_global_device_ids=true, to_apply=%region_10.11 | all-reduce | flops 384 | bytes 3072 | tf_op jit(solution)/shard_map/psum | solution.py:159
  128.0 5.3 %gather_fusion = bf16[960,1024]{1,0:T(8,128)(2,1)} fusion(bf16[385,1024]{1,0:T(8,128)(2,1)S(1)} %concatenate.13, s32[1024]{0:T(1024)S(1)} %pad_clamp_fusion.1), kind=kCustom, calls=%fused_computation | custom fusion | bytes 3936000 | tf_op jit(solution)/shard_map/gather | solution.py:174
  133.3 69.5 %all_to_all.10 = bf16[8,120,1024]{2,1,0:T(8,128)(2,1)} all-to-all(bf16[8,120,1024]{2,1,0:T(8,128)(2,1)} %bitcast.80), channel_id=1, replica_groups=mesh['sp'=8,'tp'=4] {'sp'}, dimensions={0} | all-to-all | bytes 3932160 | tf_op jit(solution)/shard_map/all_to_all | solution.py:175
  202.9 82.4 %all-gather.7.cloned.1.call-done = bf16[1,960,4096]{2,1,0:T(8,128)(2,1)} async-done(((bf16[1,960,1024]{2,1,0:T(8,128)(2,1)}), bf16[1,960,4096]{2,1,0:T(8,128)(2,1)}) %all-gather.7.cloned.1.call-update) | async-done | bytes 7864336 | tf_op jit(solution)/shard_map/all_gather | solution.py:180
  285.4 6.2 %fusion.28 = f32[960,256]{1,0:T(8,128)S(1)} fusion(bf16[1,960,4096]{2,1,0:T(8,128)(2,1)} %all-gather.7.cloned.1.call-done, bf16[1,4096,256]{2,1,0:T(8,128)(2,1)} %param.33), kind=kOutput, calls=%fused_computation.37 | convolution fusion | flops 2013265920 | bytes 10944512 | tf_op jit(solution)/shard_map/erd,edf->erf/dot_general | solution.py:181
  295.1 34.1 %all-gather.9.cloned.1.call-done = bf16[960,1024]{1,0:T(8,128)(2,1)} async-done(((bf16[960,256]{1,0:T(8,128)(2,1)}), bf16[960,1024]{1,0:T(8,128)(2,1)}) %all-gather.9.cloned.1.call-update) | async-done | bytes 1966096 | tf_op jit(solution)/shard_map/all_gather | solution.py:186
  329.2 5.0 %fusion.34 = bf16[960,1024]{1,0:T(8,128)(2,1)} fusion(bf16[960,1024]{1,0:T(8,128)(2,1)} %all-gather.9.cloned.1.call-done, bf16[1,1024,1024]{2,1,0:T(8,128)(2,1)S(1)} %copy-done), kind=kOutput, calls=%fused_computation.47 | convolution fusion | flops 2014248960 | bytes 6029312 | tf_op jit(solution)/shard_map/erf,efd->erd/dot_general | solution.py:184
  334.2 5.7 %all-to-all-start.1 = ((bf16[8,120,1024]{2,1,0:T(8,128)(2,1)}), bf16[8,120,1024]{2,1,0:T(8,128)(2,1)}, u32[]{:S(2)}, u32[]{:S(2)}) async-start(bf16[8,120,1024]{2,1,0:T(8,128)(2,1)} %bitcast.82), calls=%async_computation.1 | async-start | bytes 3932160 | tf_op jit(solution)/shard_map/all_to_all | solution.py:192
  340.1 42.6 %all-to-all-done.1 = bf16[8,120,1024]{2,1,0:T(8,128)(2,1)} async-done(((bf16[8,120,1024]{2,1,0:T(8,128)(2,1)}), bf16[8,120,1024]{2,1,0:T(8,128)(2,1)}, u32[]{:S(2)}, u32[]{:S(2)}) %all-to-all-start.1) | async-done | bytes 1966112 | tf_op jit(solution)/shard_map/all_to_all | solution.py:192
  382.6 6.4 %gather_fusion.1 = bf16[768,1024]{1,0:T(8,128)(2,1)} fusion(bf16[960,1024]{1,0:T(8,128)(2,1)} %bitcast.21, s32[1024]{0:T(1024)S(1)} %pad_clamp_fusion), kind=kCustom, calls=%fused_computation.1 | custom fusion | bytes 3148800 | tf_op jit(solution)/shard_map/gather | solution.py:193
  389.0 4.7 %reshape.223 = f32[384,2,1024]{2,1,0:T(2,128)} reshape(bf16[768,1024]{1,0:T(8,128)(2,1)} %gather_fusion.1) | data formatting | bytes 4718592 | tf_op jit(solution)/shard_map/convert_element_type | solution.py:195
  393.7 5.9 %multiply_reduce_fusion = f32[384,1024]{1,0:T(8,128)S(1)} fusion(f32[384,2,1024]{2,1,0:T(2,128)} %reshape.223, f32[384,2]{1,0:T(8,128)S(1)} %copy.43), kind=kLoop, calls=%fused_computation.39 | loop fusion | flops 1179648 | bytes 4721664 | tf_op jit(solution)/shard_map/reduce_sum | solution.py:197
  (103 shorter events, 46.0 us)
Async XLA Ops:
  6.5 322.6 %copy-start = (bf16[1,1024,1024]{2,1,0:T(8,128)(2,1)S(1)}, bf16[1,1024,1024]{2,1,0:T(8,128)(2,1)}, u32[]{:S(2)}) copy-start(bf16[1,1024,1024]{2,1,0:T(8,128)(2,1)} %param.35) | copy-start | bytes 6291460
  6.5 6.8 %copy-start.6 = (s32[384,2]{0,1:T(2,128)S(1)}, s32[384,2]{0,1:T(2,128)}, u32[]{:S(2)}) copy-start(s32[384,2]{0,1:T(2,128)} %param.31) | copy-start | bytes 9220
  6.5 4.5 %copy-start.5 = (bf16[384,32]{0,1:T(8,128)(2,1)S(1)}, bf16[384,32]{0,1:T(8,128)(2,1)}, u32[]{:S(2)}) copy-start(bf16[384,32]{0,1:T(8,128)(2,1)} %param.25) | copy-start | bytes 73732
  6.5 4.5 %copy-start.4 = (bf16[384,128]{1,0:T(8,128)(2,1)S(1)}, bf16[384,128]{1,0:T(8,128)(2,1)}, u32[]{:S(2)}) copy-start(bf16[384,128]{1,0:T(8,128)(2,1)} %param.23) | copy-start | bytes 294916
  6.5 43.6 %copy-start.3 = (bf16[384,256]{1,0:T(8,128)(2,1)S(1)}, bf16[384,256]{1,0:T(8,128)(2,1)}, u32[]{:S(2)}) copy-start(bf16[384,256]{1,0:T(8,128)(2,1)} %param.22) | copy-start | bytes 589828
  6.5 43.6 %copy-start.11 = (bf16[512,256]{1,0:T(8,128)(2,1)S(1)}, bf16[512,256]{1,0:T(8,128)(2,1)}, u32[]{:S(2)}) copy-start(bf16[512,256]{1,0:T(8,128)(2,1)} %param.27) | copy-start | bytes 786436
  6.6 43.6 %copy-start.12 = (bf16[512,256]{1,0:T(8,128)(2,1)S(1)}, bf16[512,256]{1,0:T(8,128)(2,1)}, u32[]{:S(2)}) copy-start(bf16[512,256]{1,0:T(8,128)(2,1)} %param.28) | copy-start | bytes 786436
  6.6 43.6 %all-gather.5.cloned.1.call-start = ((), (), s32[]{:S(2)}) async-start(), calls=%async_computation.2 | async-start | bytes 3538944 | tf_op jit(solution)/shard_map/all_gather | solution.py:125
  9.9 275.5 %all-gather.7.cloned.1.call-start = ((), (), s32[]{:S(2)}) async-start(), calls=%async_computation.3 | async-start | bytes 9830400 | tf_op jit(solution)/shard_map/all_gather | solution.py:180
  117.6 10.1 %copy-start.7 = (f32[1024]{0:T(1024)S(1)}, f32[1024]{0:T(1024)}, u32[]{:S(2)}) copy-start(f32[1024]{0:T(1024)} %param.30) | copy-start | bytes 12292
  120.5 7.2 %copy-start.1 = (bf16[384,1024]{1,0:T(8,128)(2,1)}, bf16[384,1024]{1,0:T(8,128)(2,1)S(1)}, u32[]{:S(2)}) copy-start(bf16[384,1024]{1,0:T(8,128)(2,1)S(1)} %get-tuple-element.290) | copy-start | bytes 2359300
  202.9 126.3 %all-gather.9.cloned.1.call-start = ((), (), s32[]{:S(2)}) async-start(), calls=%async_computation.4 | async-start | bytes 2457600 | tf_op jit(solution)/shard_map/all_gather | solution.py:186
  285.4 6.2 %copy-start.9 = (bf16[1,960,4096]{2,1,0:T(8,128)(2,1)S(1)}, bf16[1,960,4096]{2,1,0:T(8,128)(2,1)}, u32[]{:S(2)}) copy-start(bf16[1,960,4096]{2,1,0:T(8,128)(2,1)} %all-gather.7.cloned.1.call-done) | copy-start | bytes 23592964
  285.4 6.7 %copy-start.10 = (bf16[1,4096,256]{2,1,0:T(8,128)(2,1)S(1)}, bf16[1,4096,256]{2,1,0:T(8,128)(2,1)}, u32[]{:S(2)}) copy-start(bf16[1,4096,256]{2,1,0:T(8,128)(2,1)} %param.34) | copy-start | bytes 6291460
  334.2 5.7 %copy-start.8 = (f32[384,2]{0,1:T(2,128)S(1)}, f32[384,2]{0,1:T(2,128)}, u32[]{:S(2)}) copy-start(f32[384,2]{0,1:T(2,128)} %param.32) | copy-start | bytes 9220
  334.2 48.5 %all-to-all-start.1 = ((bf16[8,120,1024]{2,1,0:T(8,128)(2,1)}), bf16[8,120,1024]{2,1,0:T(8,128)(2,1)}, u32[]{:S(2)}, u32[]{:S(2)}) async-start(bf16[8,120,1024]{2,1,0:T(8,128)(2,1)} %bitcast.82), calls=%async_computation.1 | async-start | bytes 3932160 | tf_op jit(solution)/shard_map/all_to_all | solution.py:192
  393.7 6.0 %copy-start.2 = (bf16[384,1024]{1,0:T(8,128)(2,1)S(1)}, bf16[384,1024]{1,0:T(8,128)(2,1)}, u32[]{:S(2)}) copy-start(bf16[384,1024]{1,0:T(8,128)(2,1)} %copy-done.1) | copy-start | bytes 2359300
Sparse Core Ops, SparseCore 0:
  10.0 40.1 all-gather.4
  203.0 82.2 all-gather.6
  295.2 33.9 all-gather.8
where the time goes:
time: 413 us; the launch traced here: 407 us
  waiting for transfers between devices  176 us (43%)
  blocking collectives  104 us (25%)
  local copies, waits for them, and re-layouts  48.8 us (12%)
  matrix products  37.1 us (9%)
  other arithmetic  20 us (5%)
  between operations  13.4 us (3%)
  starting transfers between devices  5.84 us (1%)
    all_gather x1, waiting for transfers between devices, per_device(): pieces = lax.all_gather(grouped, 'tp', axis=2, tiled=True)  82.4 us
    all_to_all x1, blocking collectives, per_device(): lax.all_to_all(send_rows, 'sp', split_axis=0, concat_axis=0, tiled=True)  69.5 us
    all_to_all x1, waiting for transfers between devices, per_device(): lax.all_to_all(result, 'sp', split_axis=0, concat_axis=0, tiled=True)  42.6 us
    all_gather x1, waiting for transfers between devices, per_device(): lax.all_gather(hidden, 'tp', axis=2, tiled=True)  34.1 us
    all_gather x1, waiting for transfers between devices, per_device(): lat_piece = lax.all_gather(lat_norm, 'sp', axis=0, tiled=True)  16.7 us
    all_gather x1, blocking collectives, per_device(): rope_piece = lax.all_gather(rot_key, 'sp', axis=0, tiled=True)  16 us
    all_gather x1, blocking collectives, per_device(): lax.all_gather(attended, 'tp', axis=1, tiled=True)  10.9 us
    while x2, local copies, waits for them, and re-layouts, absorb(): carried, _ = lax.scan(stepper, carried, blocks)  10.8 us
  transfers between devices with their start and end apart: 4, of which 4 were waited for; matrix products, arithmetic and copies ran while one was open for 2% of the time, Pallas kernels for 0%

commit v1 on v0

v1 whole, which is shorter than its diff:
```python
import functools

import jax
import jax.numpy as jnp
from jax import lax
from jax.experimental import pallas as pl
from jax.experimental.pallas import tpu as pltpu
from jax.sharding import PartitionSpec as P

NOPE_DIM = 64
ROPE_DIM = 32
VALUE_DIM = 64
TOP_K = 2
LANES = 128

epsilon = 1e-06
rope_base = 10000.0
negative = -1e30
MESH = pl.DeviceIdType.MESH
bf16 = jnp.bfloat16
f32 = jnp.float32


def rotate(values_in, places):
    half_dim = values_in.shape[-1] // 2
    inverse = rope_base ** (-jnp.arange(half_dim, dtype=jnp.float32) / half_dim)
    angles = places.astype(jnp.float32)[:, None] * inverse[None, :]
    angles = angles.reshape((angles.shape[0],) + (1,) * (values_in.ndim - 2) + (half_dim,))
    cosine = jnp.cos(angles)
    sine_wave = jnp.sin(angles)
    first_half = values_in[..., :half_dim]
    second_half = values_in[..., half_dim:]
    return jnp.concatenate(
        [
            first_half * cosine - second_half * sine_wave,
            first_half * sine_wave + second_half * cosine,
        ],
        axis=-1,
    )


def norm_rows(values_in, gain_vec):
    wide = values_in.astype(jnp.float32)
    mean_square = jnp.mean(wide * wide, axis=-1, keepdims=True)
    return (wide * lax.rsqrt(mean_square + epsilon) * gain_vec[None, :]).astype(jnp.bfloat16)


def flip(a, b, n):
    total = 0
    bit = 1
    while bit < n:
        total = total + ((a // bit) % 2 + (b // bit) % 2) % 2 * bit
        bit *= 2
    return total


def attend_kernel(heads, q_ref, lat_ref, wk_ref, wv_ref, out_ref, top_ref, acc_ref):
    rows = q_ref.shape[0]
    me = lax.axis_index("sp")
    scale = (NOPE_DIM + ROPE_DIM) ** (-0.5) * 1.4426950408889634
    top_ref[...] = jnp.full(top_ref.shape, negative, f32)
    acc_ref[...] = jnp.zeros(acc_ref.shape, f32)

    def block(b, masked):
        lat = lat_ref[pl.ds(pl.multiple_of(b * rows, rows), rows), :]
        keys = jnp.dot(lat, wk_ref[...], preferred_element_type=f32).astype(bf16)
        values = jnp.dot(lat, wv_ref[...], preferred_element_type=f32).astype(bf16)
        for h in range(heads):
            cols = slice(h * LANES, (h + 1) * LANES)
            scores = lax.dot_general(
                q_ref[:, cols], keys[:, cols], (((1,), (1,)), ((), ())), preferred_element_type=f32
            )
            if masked:
                allowed = lax.broadcasted_iota(jnp.int32, scores.shape, 1) <= (
                    lax.broadcasted_iota(jnp.int32, scores.shape, 0)
                )
                scores = jnp.where(allowed, scores, negative)
            old = top_ref[h]
            new = jnp.maximum(old, jnp.max(scores, axis=1, keepdims=True))
            weights = jnp.exp2((scores - new[:, :1]) * scale)
            fading = jnp.exp2((old - new) * scale)
            top_ref[h] = new
            acc_ref[h] = acc_ref[h] * fading + jnp.dot(
                weights.astype(bf16), values[:, cols], preferred_element_type=f32
            )

    @pl.loop(0, me)
    def _(b):
        block(b, False)

    block(me, True)
    outs = []
    for h in range(heads):
        acc = acc_ref[h]
        outs.append(acc[:, :VALUE_DIM] / acc[:, VALUE_DIM : VALUE_DIM + 1])
    out_ref[...] = jnp.concatenate(outs, axis=1).astype(bf16)


def expert_kernel(
    S, T, C, M,
    att_ref, res_ref, wo_ref, gain_ref, slot_ref, cols_ref, *rest,
):
    w_hbm = rest[:T]
    down_hbm = rest[T]
    out_ref = rest[T + 1]
    (
        att_all, sq_own, sq_all, mid_ref, acc_ref, norm_ref, send, recv, psend, precv, own, hid, res, ret,
        w_ref, down_ref,
        load_sem, att_s, att_r, sq_s, sq_r, d_s, d_r, p_s, p_r, h_s, h_r, r_s, r_r,
    ) = rest[T + 2 :]
    me_s = lax.axis_index("sp")
    me_t = lax.axis_index("tp")
    rows, K = res_ref.shape
    heads_w = att_ref.shape[1]
    F = w_ref.shape[2] // 2

    loads = [pltpu.make_async_copy(w_hbm[d], w_ref.at[d], load_sem.at[d]) for d in range(T)]
    loads.append(pltpu.make_async_copy(down_hbm, down_ref, load_sem.at[T]))

    barrier = pltpu.get_barrier_semaphore()
    for d in range(1, T):
        pl.semaphore_signal(barrier, inc=1, device_id=(me_s, flip(me_t, d, T)), device_id_type=MESH)
    for j in range(1, S):
        pl.semaphore_signal(barrier, inc=1, device_id=(flip(me_s, j, S), me_t), device_id_type=MESH)
    pl.semaphore_wait(barrier, S + T - 2)

    def remote(src, dst, ss, rs, s, t):
        return pltpu.make_async_remote_copy(
            src_ref=src, dst_ref=dst, send_sem=ss, recv_sem=rs, device_id=(s, t), device_id_type=MESH
        )

    def att_copy(d):
        return remote(att_ref, att_all.at[d - 1], att_s.at[d - 1], att_r.at[d - 1], me_s, flip(me_t, d, T))

    def sq_copy(d):
        return remote(sq_own, sq_all.at[d - 1], sq_s.at[d - 1], sq_r.at[d - 1], me_s, flip(me_t, d, T))

    def d_copy(j):
        return remote(send.at[j], recv.at[j], d_s.at[j], d_r.at[j], flip(me_s, j, S), me_t)

    def p_copy(j, d):
        return remote(
            psend.at[j, d - 1], precv.at[j, d - 1], p_s.at[j % M, d - 1], p_r.at[j % M, d - 1],
            me_s, flip(me_t, d, T),
        )

    def h_copy(j, d):
        return remote(
            hid.at[j, 0], hid.at[j, d], h_s.at[j % M, d - 1], h_r.at[j % M, d - 1], me_s, flip(me_t, d, T)
        )

    def r_copy(j):
        return remote(res.at[j], ret.at[j], r_s.at[j], r_r.at[j], flip(me_s, j, S), me_t)

    for d in range(1, T):
        att_copy(d).start()
    for load in loads:
        load.start()

    def project(att, d):
        begin = pl.multiple_of(flip(me_t, d, T) * heads_w, heads_w)
        return jnp.dot(att, wo_ref[pl.ds(begin, heads_w), :], preferred_element_type=f32)

    acc_ref[...] = res_ref[...].astype(f32) + project(att_ref[...], 0)
    for d in range(1, T):
        att_copy(d).wait_recv()
        acc_ref[...] += project(att_all[d - 1], d)
    mid_ref[...] = acc_ref[...].astype(bf16)
    wide = mid_ref[...].astype(f32)
    square = jnp.sum(wide * wide, axis=1, keepdims=True)
    sq_own[...] = jnp.transpose(jnp.broadcast_to(square, (rows, LANES)))[:8]
    for d in range(1, T):
        sq_copy(d).start()
    total = sq_own[...]
    for d in range(1, T):
        sq_copy(d).wait_recv()
        total = total + sq_all[d - 1]
    row_scale = lax.rsqrt(total / (K * T) + epsilon)
    row_scale = jnp.transpose(jnp.broadcast_to(row_scale[:1], (LANES, rows)))[:, :1]
    wide = mid_ref[...].astype(f32)
    norm_ref[...] = (wide * row_scale * gain_ref[...]).astype(bf16)
    acc_ref[...] = wide

    def rows_for(j):
        base = (flip(me_s, j, S) * C).astype(f32)
        places = lax.broadcasted_iota(jnp.int32, (C, rows), 0).astype(f32) + base
        hit = (places == slot_ref[0:1, :]) | (places == slot_ref[1:2, :])
        picks = jnp.where(hit, 1.0, 0.0).astype(bf16)
        return jnp.dot(picks, norm_ref[...], preferred_element_type=f32).astype(bf16)

    @pl.loop(1, S)
    def _(j):
        send[j] = rows_for(j)
        d_copy(j).start()

    recv[0] = rows_for(0)
    for load in loads:
        load.wait()

    def add_result(j):
        base = (flip(me_s, j, S) * C).astype(f32)
        places = lax.broadcasted_iota(jnp.int32, (rows, C), 1).astype(f32) + base
        hit0 = places == cols_ref[:, 0:1]
        hit1 = places == cols_ref[:, 1:2]
        picks = jnp.where(hit0 | hit1, 1.0, 0.0).astype(bf16)
        inside0 = (cols_ref[:, 0:1] >= base) & (cols_ref[:, 0:1] < base + C)
        inside1 = (cols_ref[:, 1:2] >= base) & (cols_ref[:, 1:2] < base + C)
        share = jnp.where(inside0, cols_ref[:, 2:3], jnp.where(inside1, cols_ref[:, 3:4], 0.0))
        acc_ref[...] += share * jnp.dot(picks, ret[j], preferred_element_type=f32)

    @pl.loop(0, S + 2)
    def _(i):
        @pl.when(i < S)
        def _():
            j = i

            @pl.when(j > 0)
            def _():
                d_copy(j).wait_recv()

            block = recv[j]
            for d in range(1, T):
                if S > M:

                    @pl.when(j >= M)
                    def _():
                        p_copy(j - M, d).wait_send()

                psend[j, d - 1] = jnp.dot(block, w_ref[d], preferred_element_type=f32).astype(bf16)
                p_copy(j, d).start()
            own[j % 2] = jnp.dot(block, w_ref[0], preferred_element_type=f32)

        @pl.when((i >= 1) & (i < S + 1))
        def _():
            j = i - 1
            total = own[j % 2]
            for d in range(1, T):
                p_copy(j, d).wait_recv()
                total = total + precv[j, d - 1].astype(f32)
            gate = total[:, :F]
            hid[j, 0] = (gate / (1.0 + jnp.exp(-gate)) * total[:, F:]).astype(bf16)
            for d in range(1, T):
                if S > M:

                    @pl.when(j >= M)
                    def _():
                        h_copy(j - M, d).wait_send()

                h_copy(j, d).start()

        @pl.when(i >= 2)
        def _():
            j = i - 2
            total = jnp.zeros((C, K), f32)
            for d in range(T):
                if d > 0:
                    h_copy(j, d).wait_recv()
                begin = pl.multiple_of(flip(me_t, d, T) * F, F)
                total += jnp.dot(hid[j, d], down_ref[pl.ds(begin, F), :], preferred_element_type=f32)

            @pl.when(j > 0)
            def _():
                res[j] = total.astype(bf16)
                r_copy(j).start()

            @pl.when(j == 0)
            def _():
                ret[j] = total.astype(bf16)

    add_result(0)

    @pl.loop(1, S)
    def _(j):
        r_copy(j).wait_recv()
        add_result(j)

    out_ref[...] = acc_ref[...].astype(bf16)

    for d in range(1, T):
        att_copy(d).wait_send()
        sq_copy(d).wait_send()

    @pl.loop(S - M, S)
    def _(j):
        for d in range(1, T):
            p_copy(j, d).wait_send()
            h_copy(j, d).wait_send()

    @pl.loop(1, S)
    def _(j):
        d_copy(j).wait_send()
        r_copy(j).wait_send()


def per_device(
    residual, query_nope, query_rope, latent, key_rope, latent_gain, key_up, value_up, out_proj,
    norm_gain, routes, route_weight, expert_gate, expert_up, expert_down,
):
    rows, K = residual.shape
    S = lax.axis_size("sp")
    T = lax.axis_size("tp")
    me_s = lax.axis_index("sp")
    me_t = lax.axis_index("tp")
    heads = query_nope.shape[1] // NOPE_DIM
    rank = latent.shape[1]
    F = expert_gate.shape[2]

    width = -(-(rank + ROPE_DIM + 1) // LANES) * LANES
    places = me_s * rows + jnp.arange(rows, dtype=jnp.int32)
    part = rows // T
    begin = me_t * part
    my_places = lax.dynamic_slice(places, (begin,), (part,))
    my_latent = norm_rows(lax.dynamic_slice(latent, (begin, 0), (part, rank)), latent_gain)
    my_rope = rotate(
        lax.dynamic_slice(key_rope, (begin, 0), (part, ROPE_DIM)).astype(f32), my_places
    ).astype(bf16)
    packed = jnp.concatenate(
        [
            my_latent,
            my_rope,
            jnp.ones((part, 1), bf16),
            jnp.zeros((part, width - rank - ROPE_DIM - 1), bf16),
        ],
        axis=1,
    )
    latents = lax.all_gather(packed, ("sp", "tp"), axis=0, tiled=True)

    both = []
    for d in range(T):
        other = me_t ^ d
        piece = jnp.concatenate(
            [
                lax.dynamic_slice(expert_gate[0], (other * K, 0), (K, F)),
                lax.dynamic_slice(expert_up[0], (other * K, 0), (K, F)),
            ],
            axis=1,
        )
        if d > 0:
            piece = lax.ppermute(piece, "tp", [(i, i ^ d) for i in range(T)])
        both.append(piece)

    rot_query = rotate(
        query_rope.astype(f32).reshape(rows, heads, ROPE_DIM), places
    ).astype(bf16)
    query = jnp.concatenate(
        [
            query_nope.reshape(rows, heads, NOPE_DIM),
            rot_query,
            jnp.zeros((rows, heads, LANES - NOPE_DIM - ROPE_DIM), bf16),
        ],
        axis=2,
    ).reshape(rows, heads * LANES)
    rope_in = jnp.zeros((width - rank, LANES), bf16)
    rope_in = rope_in + jnp.asarray(
        jnp.arange(width - rank)[:, None] + NOPE_DIM == jnp.arange(LANES)[None, :]
    ).astype(bf16) * (jnp.arange(width - rank)[:, None] < ROPE_DIM).astype(bf16)
    one_in = (
        (jnp.arange(width - rank)[:, None] == ROPE_DIM)
        & (jnp.arange(LANES)[None, :] == VALUE_DIM)
    ).astype(bf16)

    def widen(weight, size, tail):
        weight = weight.reshape(rank, heads, size)
        weight = jnp.pad(weight, ((0, 0), (0, 0), (0, LANES - size))).reshape(rank, heads * LANES)
        return jnp.concatenate([weight, jnp.tile(tail, (1, heads))], axis=0)

    wk = widen(key_up, NOPE_DIM, rope_in)
    wv = widen(value_up, VALUE_DIM, one_in)
    vmem = pl.BlockSpec(memory_space=pltpu.VMEM)
    seq = S * rows
    attended = pl.pallas_call(
        functools.partial(attend_kernel, heads),
        name="attend",
        out_shape=jax.ShapeDtypeStruct((rows, heads * VALUE_DIM), bf16),
        in_specs=[vmem] * 4,
        out_specs=vmem,
        scratch_shapes=[
            pltpu.VMEM((heads, rows, LANES), f32),
            pltpu.VMEM((heads, rows, LANES), f32),
        ],
        compiler_params=pltpu.CompilerParams(vmem_limit_bytes=48 * 2**20),
        cost_estimate=pl.CostEstimate(
            flops=4 * heads * rows * seq * LANES + 4 * seq * width * heads * LANES,
            bytes_accessed=seq * width * 2,
            transcendentals=heads * rows * seq,
        ),
    )(query, latents, wk, wv)

    experts = S * expert_gate.shape[0]
    capacity = 5 * rows * TOP_K // (4 * experts)
    C = -(-capacity // 8) * 8
    M = min(S, 8 if T <= 4 else 4)
    chosen = routes[:, :, None] == jnp.arange(experts, dtype=jnp.int32)[None, None, :]
    named = jnp.sum(chosen.astype(f32), axis=1).astype(bf16)
    earlier = (jnp.arange(rows)[:, None] > jnp.arange(rows)[None, :]).astype(bf16)
    before = jnp.dot(earlier, named, preferred_element_type=f32)
    number = jnp.sum(jnp.where(chosen, before[:, None, :], 0.0), axis=2)
    slots = routes.astype(f32) * C + number
    slot_rows = jnp.transpose(slots)
    slot_cols = jnp.concatenate([slots, route_weight], axis=1)

    anywhere = pl.BlockSpec(memory_space=pl.ANY)
    dma = pltpu.SemaphoreType.DMA
    return pl.pallas_call(
        functools.partial(expert_kernel, S, T, C, M),
        name="experts",
        out_shape=jax.ShapeDtypeStruct((rows, K), bf16),
        in_specs=[vmem] * 6 + [anywhere] * (T + 1),
        out_specs=vmem,
        scratch_shapes=[
            pltpu.VMEM((T - 1, rows, heads * VALUE_DIM), bf16),
            pltpu.VMEM((8, rows), f32),
            pltpu.VMEM((T - 1, 8, rows), f32),
            pltpu.VMEM((rows, K), bf16),
            pltpu.VMEM((rows, K), f32),
            pltpu.VMEM((rows, K), bf16),
            pltpu.VMEM((S, C, K), bf16),
            pltpu.VMEM((S, C, K), bf16),
            pltpu.VMEM((S, T - 1, C, 2 * F), bf16),
            pltpu.VMEM((S, T - 1, C, 2 * F), bf16),
            pltpu.VMEM((2, C, 2 * F), f32),
            pltpu.VMEM((S, T, C, F), bf16),
            pltpu.VMEM((S, C, K), bf16),
            pltpu.VMEM((S, C, K), bf16),
            pltpu.VMEM((T, K, 2 * F), bf16),
            pltpu.VMEM(expert_down.shape[1:], bf16),
            dma((T + 1,)),
            dma((T - 1,)), dma((T - 1,)), dma((T - 1,)), dma((T - 1,)),
            dma((S,)), dma((S,)),
            dma((M, T - 1)), dma((M, T - 1)), dma((M, T - 1)), dma((M, T - 1)),
            dma((S,)), dma((S,)),
        ],
        compiler_params=pltpu.CompilerParams(
            collective_id=0, has_side_effects=True, vmem_limit_bytes=56 * 2**20
        ),
        cost_estimate=pl.CostEstimate(
            flops=6 * S * C * K * F * T, bytes_accessed=8 * K * K * 2, transcendentals=S * C * F
        ),
    )(attended, residual, out_proj, norm_gain[None, :], slot_rows, slot_cols, *both, expert_down[0])


def solution(mesh):
    in_specs = (
        P("sp", "tp"),
        P("sp", "tp"),
        P("sp", "tp"),
        P("sp", None),
        P("sp", None),
        P(),
        P(None, "tp"),
        P(None, "tp"),
        P(None, "tp"),
        P("tp"),
        P("sp", None),
        P("sp", None),
        P("sp", None, "tp"),
        P("sp", None, "tp"),
        P("sp", None, "tp"),
    )
    out_specs = P("sp", "tp")
    return jax.shard_map(
        per_device, mesh=mesh, in_specs=in_specs, out_specs=out_specs, check_vma=False
    )
```

time: 413 us -> 230 us (0.56); the launches traced: 407 us -> 229 us
  Pallas kernels: 0 us -> 135 us
  waiting for transfers between devices: 176 us -> 59.8 us
  blocking collectives: 104 us -> 0 us
  local copies, waits for them, and re-layouts: 48.8 us -> 10.7 us
  matrix products: 37.1 us -> 0.13 us
  other arithmetic: 20 us -> 7.44 us
    pallas_call x0 -> x2, Pallas kernels: none -> 135 us  [the longest x1 122 us: per_device(): pl.pallas_call(functools.partial(expert_kernel, S, T, C, M), name='expert...]
    all_gather x3 -> x1, waiting for transfers between devices: 133 us -> 59.7 us  [per_device(): latents = lax.all_gather(packed, ('sp', 'tp'), axis=0, tiled=True)]
    all_to_all x1 -> x0, blocking collectives: 69.5 us -> none  [per_device(): lax.all_to_all(send_rows, 'sp', split_axis=0, concat_axis=0, tiled=True)]
    all_to_all x1 -> x0, waiting for transfers between devices: 42.6 us -> none  [per_device(): lax.all_to_all(result, 'sp', split_axis=0, concat_axis=0, tiled=True)]
    dot_general x12 -> x1, matrix products: 37.1 us -> 0.13 us  [per_device(): before = jnp.dot(earlier, named, preferred_element_type=f32)]
    all_gather x2 -> x0, blocking collectives: 26.9 us -> none  [the longest x1 16 us: per_device(): rope_piece = lax.all_gather(rot_key, 'sp', axis=0, tiled=True)]
    gather x2 -> x0, local copies, waits for them, and re-layouts: 11.6 us -> none  [the longest x1 6.35 us: per_device(): gathered = returned.reshape(experts_all * capacity, columns)[slot_index]]
    reshape x4 -> x3, local copies, waits for them, and re-layouts: 11.6 us -> 0.62 us  [the longest x2 0.43 us: widen(): jnp.pad(weight, ((0, 0), (0, 0), (0, LANES - size)))]
  transfers between devices with their start and end apart: 4 -> 4, of which waited for: 4 -> 1; matrix products, arithmetic and copies ran while one was open for 2% -> 4% of each run, Pallas kernels for 0% -> 5%
where the time goes in v1:
time: 230 us; the launch traced here: 229 us
  Pallas kernels  135 us (59%)
  waiting for transfers between devices  59.8 us (26%)
  between operations  13.7 us (6%)
  local copies, waits for them, and re-layouts  10.7 us (5%)
  other arithmetic  7.44 us (3%)
  starting transfers between devices  2.65 us (1%)
    pallas_call x1, Pallas kernels, per_device(): pl.pallas_call(functools.partial(expert_kernel, S, T, C, M), name='expert...  122 us
    all_gather x1, waiting for transfers between devices, per_device(): latents = lax.all_gather(packed, ('sp', 'tp'), axis=0, tiled=True)  59.7 us
    pallas_call x1, Pallas kernels, per_device(): pl.pallas_call(functools.partial(attend_kernel, heads), name='attend', ou...  12.3 us
    unnamed x28, local copies, waits for them, and re-layouts  5.75 us
  transfers between devices with their start and end apart: 4, of which 1 were waited for; matrix products, arithmetic and copies ran while one was open for 4% of the time, Pallas kernels for 5%

profile of v1, /device:TPU:9, one launch (start us, length us, event | category | flops | bytes accessed | tf_op | source)
XLA Modules:
  0.0 229.1 jit_solution(13036998719965160176)
XLA Ops:
  6.6 1.0 fusion.1
  7.9 1.0 fusion.3
  8.9 0.3 fusion.12
  9.2 0.8 concatenate.34
  10.0 2.4 %dynamic-slice_bitcast_fusion = (bf16[1024,256]{1,0:T(8,128)(2,1)S(1)}, bf16[1024,256]{1,0:T(8,128)(2,1)S(1)}, bf16[1024,256]{1,0:T(8,128)(2,1)S(1)}, bf16[1024,...) fusion(bf16[1,4096,256]{2,1,0:T(8,128)(2,1)} %param.28, ...), kind=kLoop, calls=%fused_computation.8 | loop fusion | bytes 8388624 | tf_op jit(solution)/shard_map/dynamic_slice | solution.py:334
  12.4 1.1 pad_maximum_fusion.1
  13.6 1.2 collective-permute-start
  14.8 1.0 pad_maximum_fusion.2
  15.9 1.2 collective-permute-start.1
  17.1 1.1 pad_maximum_fusion.3
  18.2 0.2 collective-permute-start.2
  18.5 0.2 copy.57
  19.2 0.2 multiply_cosine_fusion.1
  19.6 0.2 copy.67.q_ref
  20.1 0.2 copy.68
  20.7 0.2 copy.69
  21.0 0.8 copy.66.cols_ref
  21.9 1.1 pad_maximum_fusion.rest_0_
  23.0 59.7 %all-gather.2.cloned.1.call-done.lat_ref = bf16[3072,640]{1,0:T(8,128)(2,1)} async-done(((bf16[96,640]{1,0:T(8,128)(2,1)}), bf16[3072,640]{1,0:T(8,128)(2,1)}) %all-gather.2.cloned.1.call-update) | async-done | bytes 3932176 | tf_op jit(solution)/shard_map/all_gather | solution.py:326
  82.7 2.1 copy-done.1
  84.8 12.3 %attend.1.att_ref = bf16[384,256]{1,0:T(8,128)(2,1)S(1)} custom-call(bf16[384,512]{1,0:T(8,128)(2,1)S(1)} %copy.67.q_ref, bf16[3072,640]{1,0:T(8,128)(2,1)S(1)} %copy-done.1, bf16[640,512]{1,0:T(8,128)(2,1)S(1)} %pad_maximum_fusion.4.wk_ref, bf16[640,512]{1,0:T(8,128)(2,1)S(1)} %pad_maximum_fusion.5.wv_ref), custom_call_target="tpu_custom_call" | custom-call | flops 6442450944 | bytes 3932160 | tf_op jit(solution)/shard_map/attend/pallas_call | solution.py:371
  97.1 0.7 copy-done.2
  97.8 122.3 %experts.1 = bf16[384,1024]{1,0:T(8,128)(2,1)} custom-call(bf16[384,256]{1,0:T(8,128)(2,1)} %copy-done.2, bf16[384,1024]{1,0:T(8,128)(2,1)} %res_ref.1, bf16[1024,1024]{1,0:T(8,128)(2,1)} %wo_ref.1, f32[1,1024]{1,0:T(1,128)} %bitcast.49, f32[2,384]{1,0:T(2,128)} %bitcast.47, f32[384,4]{1,0:T(8,128)} %copy.66.cols_ref, ...), custom_call_target="tpu_custom_call" | custom-call | flops 6039797760 | bytes 16777216 | tf_op jit(solution)/shard_map/experts/pallas_call | solution.py:404
  220.2 2.1 copy.78
  (58 shorter events, 1.9 us)
Async XLA Ops:
  6.5 1.1 copy-start
  6.5 76.2 %all-gather.2.cloned.1.call-start = ((), (), s32[]{:S(2)}) async-start(), calls=%async_computation | async-start | bytes 4055040 | tf_op jit(solution)/shard_map/all_gather | solution.py:326
  13.6 84.2 %collective-permute-start = (bf16[1024,512]{1,0:T(8,128)(2,1)}, bf16[1024,512]{1,0:T(8,128)(2,1)}, u32[]{:S(2)}, u32[]{:S(2)}) collective-permute-start(bf16[1024,512]{1,0:T(8,128)(2,1)} %pad_maximum_fusion.1), channel_id=1, source_target_pairs={{0,1},{1,0},{2,3},{3,2},{4,5},{5,4},{6,7},{7,6},{8,9},{9,8},{10,11... | collective-permute-start | bytes 3145736 | tf_op jit(solution)/shard_map/ppermute | solution.py:339
  14.8 3.6 %copy-start.6 = (bf16[384,128]{1,0:T(8,128)(2,1)S(1)}, bf16[384,128]{1,0:T(8,128)(2,1)}, u32[]{:S(2)}) copy-start(bf16[384,128]{1,0:T(8,128)(2,1)} %param.17) | copy-start | bytes 294916
  14.8 3.7 %copy-start.5 = (bf16[384,256]{1,0:T(8,128)(2,1)S(1)}, bf16[384,256]{1,0:T(8,128)(2,1)}, u32[]{:S(2)}) copy-start(bf16[384,256]{1,0:T(8,128)(2,1)} %param.16) | copy-start | bytes 589828
  14.8 4.0 %copy-start.7 = (s32[384,2]{0,1:T(2,128)S(1)}, s32[384,2]{0,1:T(2,128)}, u32[]{:S(2)}) copy-start(s32[384,2]{0,1:T(2,128)} %param.25) | copy-start | bytes 9220
  15.9 82.0 %collective-permute-start.1 = (bf16[1024,512]{1,0:T(8,128)(2,1)}, bf16[1024,512]{1,0:T(8,128)(2,1)}, u32[]{:S(2)}, u32[]{:S(2)}) collective-permute-start(bf16[1024,512]{1,0:T(8,128)(2,1)} %pad_maximum_fusion.2), channel_id=1, source_target_pairs={{0,2},{1,3},{2,0},{3,1},{4,6},{5,7},{6,4},{7,5},{8,10},{9,11},{10,... | collective-permute-start | bytes 3145736 | tf_op jit(solution)/shard_map/ppermute | solution.py:339
  17.1 2.5 %copy-start.9 = (f32[384,2]{0,1:T(2,128)S(1)}, f32[384,2]{0,1:T(2,128)}, u32[]{:S(2)}) copy-start(f32[384,2]{0,1:T(2,128)} %param.26) | copy-start | bytes 9220
  18.2 1.7 copy-start.3
  18.2 79.7 %collective-permute-start.2 = (bf16[1024,512]{1,0:T(8,128)(2,1)}, bf16[1024,512]{1,0:T(8,128)(2,1)}, u32[]{:S(2)}, u32[]{:S(2)}) collective-permute-start(bf16[1024,512]{1,0:T(8,128)(2,1)} %pad_maximum_fusion.3), channel_id=1, source_target_pairs={{0,3},{1,2},{2,1},{3,0},{4,7},{5,6},{6,5},{7,4},{8,11},{9,10},{10,... | collective-permute-start | bytes 3145736 | tf_op jit(solution)/shard_map/ppermute | solution.py:339
  19.0 1.3 copy-start.8
  19.6 1.0 copy-start.4
  82.7 2.1 copy-start.1
  97.1 0.7 copy-start.2
Sparse Core Ops, SparseCore 0:
  10.2 72.4 all-gather.1

commit v2 on v1

--- a/solution.py
+++ b/solution.py
@@ -54,16 +54,129 @@
     return total
 
 
-def attend_kernel(heads, q_ref, lat_ref, wk_ref, wv_ref, out_ref, top_ref, acc_ref):
-    rows = q_ref.shape[0]
-    me = lax.axis_index("sp")
+def layer_kernel(
+    S, T, C, M, heads,
+    q_ref, lat_ref, wk_ref, wv_ref, spread_ref, res_ref, gain_ref, slot_ref, cols_ref,
+    wo_hbm, gate_hbm, up_hbm, down_hbm,
+    out_ref,
+    lat_all, top_ref, sum_ref, nume_ref, att_ref,
+    att_all, sq_own, sq_all, mid_ref, acc_ref, norm_ref, send, recv, psend, precv, own, hid, res, ret,
+    wo_ref, gate_ref, up_ref, down_ref,
+    load_sem, z_s, c_s, l_r, w_s, w_r,
+    att_s, att_r, sq_s, sq_r, d_s, d_r, p_s, p_r, h_s, h_r, r_s, r_r,
+):
+    me_s = lax.axis_index("sp")
+    me_t = lax.axis_index("tp")
+    rows, K = res_ref.shape
+    heads_w = att_ref.shape[1]
+    F = gate_ref.shape[2]
+    CORES = 2
+    me_core = me_s % CORES
+    me_z = me_s // CORES
+    last_z = S // CORES - 1
+
+    def weight_rows(d):
+        return pl.ds(pl.multiple_of(flip(me_t, d, T) * K, K), K)
+
+    loads = [
+        pltpu.make_async_copy(wo_hbm, wo_ref, load_sem.at[0]),
+        pltpu.make_async_copy(down_hbm, down_ref, load_sem.at[1]),
+        pltpu.make_async_copy(gate_hbm.at[weight_rows(0), :], gate_ref.at[0], load_sem.at[2]),
+        pltpu.make_async_copy(up_hbm.at[weight_rows(0), :], up_ref.at[0], load_sem.at[3]),
+    ]
+    for load in loads:
+        load.start()
+
+    barrier = pltpu.get_barrier_semaphore()
+    for d in range(1, T):
+        pl.semaphore_signal(barrier, inc=1, device_id=(me_s, flip(me_t, d, T)), device_id_type=MESH)
+    for j in range(1, S):
+        pl.semaphore_signal(barrier, inc=1, device_id=(flip(me_s, j, S), me_t), device_id_type=MESH)
+    pl.semaphore_wait(barrier, S + T - 2)
+
+    def remote(src, dst, ss, rs, s, t):
+        return pltpu.make_async_remote_copy(
+            src_ref=src, dst_ref=dst, send_sem=ss, recv_sem=rs, device_id=(s, t), device_id_type=MESH
+        )
+
+    def att_copy(d):
+        return remote(att_ref, att_all.at[d - 1], att_s.at[d - 1], att_r.at[d - 1], me_s, flip(me_t, d, T))
+
+    def sq_copy(d):
+        return remote(sq_own, sq_all.at[d - 1], sq_s.at[d - 1], sq_r.at[d - 1], me_s, flip(me_t, d, T))
+
+    def d_copy(j):
+        return remote(send.at[j], recv.at[j], d_s.at[j], d_r.at[j], flip(me_s, j, S), me_t)
+
+    def p_copy(j, d):
+        return remote(
+            psend.at[j, d - 1], precv.at[j, d - 1], p_s.at[j % M, d - 1], p_r.at[j % M, d - 1],
+            me_s, flip(me_t, d, T),
+        )
+
+    def h_copy(j, d):
+        return remote(
+            hid.at[j, 0], hid.at[j, d], h_s.at[j % M, d - 1], h_r.at[j % M, d - 1], me_s, flip(me_t, d, T)
+        )
+
+    def r_copy(j):
+        return remote(res.at[j], ret.at[j], r_s.at[j], r_r.at[j], flip(me_s, j, S), me_t)
+
+    def gate_copy(d):
+        return remote(
+            gate_hbm.at[weight_rows(d), :], gate_ref.at[d], w_s.at[0, d - 1], w_r.at[0, d - 1],
+            me_s, flip(me_t, d, T),
+        )
+
+    def up_copy(d):
+        return remote(
+            up_hbm.at[weight_rows(d), :], up_ref.at[d], w_s.at[1, d - 1], w_r.at[1, d - 1],
+            me_s, flip(me_t, d, T),
+        )
+
+    def own_up():
+        return remote(lat_ref, lat_all.at[me_s], z_s.at[me_s], l_r.at[me_s], me_s + CORES, me_t)
+
+    def own_across():
+        return remote(lat_ref, lat_all.at[me_s], c_s.at[me_s], l_r.at[me_s], me_s + 1, me_t)
+
+    def pass_up(b):
+        return remote(lat_all.at[b], lat_all.at[b], z_s.at[b], l_r.at[b], me_s + CORES, me_t)
+
+    def pass_across(b):
+        return remote(
+            lat_all.at[b], lat_all.at[b], c_s.at[b], l_r.at[b], me_s + 1 - 2 * me_core, me_t
+        )
+
+    @pl.when(me_z < last_z)
+    def _():
+        own_up().start()
+
+    @pl.when(me_core == 0)
+    def _():
+        own_across().start()
+
+    for d in range(1, T):
+        gate_copy(d).start()
+        up_copy(d).start()
+
     scale = (NOPE_DIM + ROPE_DIM) ** (-0.5) * 1.4426950408889634
     top_ref[...] = jnp.full(top_ref.shape, negative, f32)
-    acc_ref[...] = jnp.zeros(acc_ref.shape, f32)
-
-    def block(b, masked):
-        lat = lat_ref[pl.ds(pl.multiple_of(b * rows, rows), rows), :]
-        keys = jnp.dot(lat, wk_ref[...], preferred_element_type=f32).astype(bf16)
+    nume_ref[...] = jnp.zeros(nume_ref.shape, f32)
+    sum_ref[...] = jnp.zeros(sum_ref.shape, f32)
+    rank = lat_ref.shape[1]
+    folds = rank // ROPE_DIM
+
+    def attend(block, masked):
+        lat = block[:rows, :]
+        packed = block[rows:, :].astype(f32)
+        rope = jnp.concatenate(
+            [packed[:, q * ROPE_DIM : (q + 1) * ROPE_DIM] for q in range(folds)], axis=0
+        ).astype(bf16)
+        keys = (
+            jnp.dot(lat, wk_ref[...], preferred_element_type=f32)
+            + jnp.dot(rope, spread_ref[...], preferred_element_type=f32)
+        ).astype(bf16)
         values = jnp.dot(lat, wv_ref[...], preferred_element_type=f32).astype(bf16)
         for h in range(heads):
             cols = slice(h * LANES, (h + 1) * LANES)
@@ -80,82 +193,40 @@
             weights = jnp.exp2((scores - new[:, :1]) * scale)
             fading = jnp.exp2((old - new) * scale)
             top_ref[h] = new
-            acc_ref[h] = acc_ref[h] * fading + jnp.dot(
+            sum_ref[h] = sum_ref[h] * fading + jnp.sum(weights, axis=1, keepdims=True)
+            nume_ref[h] = nume_ref[h] * fading + jnp.dot(
                 weights.astype(bf16), values[:, cols], preferred_element_type=f32
             )
 
-    @pl.loop(0, me)
-    def _(b):
-        block(b, False)
-
-    block(me, True)
+    attend(lat_ref[...], True)
+
+    @pl.when(me_core == 1)
+    def _():
+        pass_across(me_s - 1).wait_recv()
+        attend(lat_all[me_s - 1], False)
+
+    @pl.loop(1, me_z + 1)
+    def _(k):
+        b = me_s - CORES * k
+        pass_across(b).wait_recv()
+
+        @pl.when(me_z < last_z)
+        def _():
+            pass_up(b).start()
+
+        pass_across(b).start()
+        attend(lat_all[b], False)
+        other = b + 1 - 2 * me_core
+        pass_across(other).wait_recv()
+        attend(lat_all[other], False)
+
     outs = []
     for h in range(heads):
-        acc = acc_ref[h]
-        outs.append(acc[:, :VALUE_DIM] / acc[:, VALUE_DIM : VALUE_DIM + 1])
-    out_ref[...] = jnp.concatenate(outs, axis=1).astype(bf16)
-
-
-def expert_kernel(
-    S, T, C, M,
-    att_ref, res_ref, wo_ref, gain_ref, slot_ref, cols_ref, *rest,
-):
-    w_hbm = rest[:T]
-    down_hbm = rest[T]
-    out_ref = rest[T + 1]
-    (
-        att_all, sq_own, sq_all, mid_ref, acc_ref, norm_ref, send, recv, psend, precv, own, hid, res, ret,
-        w_ref, down_ref,
-        load_sem, att_s, att_r, sq_s, sq_r, d_s, d_r, p_s, p_r, h_s, h_r, r_s, r_r,
-    ) = rest[T + 2 :]
-    me_s = lax.axis_index("sp")
-    me_t = lax.axis_index("tp")
-    rows, K = res_ref.shape
-    heads_w = att_ref.shape[1]
-    F = w_ref.shape[2] // 2
-
-    loads = [pltpu.make_async_copy(w_hbm[d], w_ref.at[d], load_sem.at[d]) for d in range(T)]
-    loads.append(pltpu.make_async_copy(down_hbm, down_ref, load_sem.at[T]))
-
-    barrier = pltpu.get_barrier_semaphore()
-    for d in range(1, T):
-        pl.semaphore_signal(barrier, inc=1, device_id=(me_s, flip(me_t, d, T)), device_id_type=MESH)
-    for j in range(1, S):
-        pl.semaphore_signal(barrier, inc=1, device_id=(flip(me_s, j, S), me_t), device_id_type=MESH)
-    pl.semaphore_wait(barrier, S + T - 2)
-
-    def remote(src, dst, ss, rs, s, t):
-        return pltpu.make_async_remote_copy(
-            src_ref=src, dst_ref=dst, send_sem=ss, recv_sem=rs, device_id=(s, t), device_id_type=MESH
-        )
-
-    def att_copy(d):
-        return remote(att_ref, att_all.at[d - 1], att_s.at[d - 1], att_r.at[d - 1], me_s, flip(me_t, d, T))
-
-    def sq_copy(d):
-        return remote(sq_own, sq_all.at[d - 1], sq_s.at[d - 1], sq_r.at[d - 1], me_s, flip(me_t, d, T))
-
-    def d_copy(j):
-        return remote(send.at[j], recv.at[j], d_s.at[j], d_r.at[j], flip(me_s, j, S), me_t)
-
-    def p_copy(j, d):
-        return remote(
-            psend.at[j, d - 1], precv.at[j, d - 1], p_s.at[j % M, d - 1], p_r.at[j % M, d - 1],
-            me_s, flip(me_t, d, T),
-        )
-
-    def h_copy(j, d):
-        return remote(
-            hid.at[j, 0], hid.at[j, d], h_s.at[j % M, d - 1], h_r.at[j % M, d - 1], me_s, flip(me_t, d, T)
-        )
-
-    def r_copy(j):
-        return remote(res.at[j], ret.at[j], r_s.at[j], r_r.at[j], flip(me_s, j, S), me_t)
-
+        outs.append(nume_ref[h][:, :VALUE_DIM] / sum_ref[h][:, :1])
+    att_ref[...] = jnp.concatenate(outs, axis=1).astype(bf16)
     for d in range(1, T):
         att_copy(d).start()
-    for load in loads:
-        load.start()
+    loads[0].wait()
 
     def project(att, d):
         begin = pl.multiple_of(flip(me_t, d, T) * heads_w, heads_w)
@@ -194,8 +265,11 @@
         d_copy(j).start()
 
     recv[0] = rows_for(0)
-    for load in loads:
+    for load in loads[1:]:
         load.wait()
+    for d in range(1, T):
+        gate_copy(d).wait_recv()
+        up_copy(d).wait_recv()
 
     def add_result(j):
         base = (flip(me_s, j, S) * C).astype(f32)
@@ -226,9 +300,15 @@
                     def _():
                         p_copy(j - M, d).wait_send()
 
-                psend[j, d - 1] = jnp.dot(block, w_ref[d], preferred_element_type=f32).astype(bf16)
+                psend[j, d - 1, :, :F] = jnp.dot(
+                    block, gate_ref[d], preferred_element_type=f32
+                ).astype(bf16)
+                psend[j, d - 1, :, F:] = jnp.dot(
+                    block, up_ref[d], preferred_element_type=f32
+                ).astype(bf16)
                 p_copy(j, d).start()
-            own[j % 2] = jnp.dot(block, w_ref[0], preferred_element_type=f32)
+            own[j % 2, :, :F] = jnp.dot(block, gate_ref[0], preferred_element_type=f32)
+            own[j % 2, :, F:] = jnp.dot(block, up_ref[0], preferred_element_type=f32)
 
         @pl.when((i >= 1) & (i < S + 1))
         def _():
@@ -276,7 +356,27 @@
 
     out_ref[...] = acc_ref[...].astype(bf16)
 
-    for d in range(1, T):
+    @pl.when(me_z < last_z)
+    def _():
+        own_up().wait_send()
+
+    @pl.when(me_core == 0)
+    def _():
+        own_across().wait_send()
+
+    @pl.loop(1, me_z + 1)
+    def _(k):
+        b = me_s - CORES * k
+
+        @pl.when(me_z < last_z)
+        def _():
+            pass_up(b).wait_send()
+
+        pass_across(b).wait_send()
+
+    for d in range(1, T):
+        gate_copy(d).wait_send()
+        up_copy(d).wait_send()
         att_copy(d).wait_send()
         sq_copy(d).wait_send()
 
@@ -305,39 +405,13 @@
     rank = latent.shape[1]
     F = expert_gate.shape[2]
 
-    width = -(-(rank + ROPE_DIM + 1) // LANES) * LANES
     places = me_s * rows + jnp.arange(rows, dtype=jnp.int32)
-    part = rows // T
-    begin = me_t * part
-    my_places = lax.dynamic_slice(places, (begin,), (part,))
-    my_latent = norm_rows(lax.dynamic_slice(latent, (begin, 0), (part, rank)), latent_gain)
-    my_rope = rotate(
-        lax.dynamic_slice(key_rope, (begin, 0), (part, ROPE_DIM)).astype(f32), my_places
-    ).astype(bf16)
+    folds = rank // ROPE_DIM
+    rot_key = rotate(key_rope.astype(f32), places).astype(bf16)
+    folded = jnp.swapaxes(rot_key.reshape(folds, rows // folds, ROPE_DIM), 0, 1)
     packed = jnp.concatenate(
-        [
-            my_latent,
-            my_rope,
-            jnp.ones((part, 1), bf16),
-            jnp.zeros((part, width - rank - ROPE_DIM - 1), bf16),
-        ],
-        axis=1,
+        [norm_rows(latent, latent_gain), folded.reshape(rows // folds, rank)], axis=0
     )
-    latents = lax.all_gather(packed, ("sp", "tp"), axis=0, tiled=True)
-
-    both = []
-    for d in range(T):
-        other = me_t ^ d
-        piece = jnp.concatenate(
-            [
-                lax.dynamic_slice(expert_gate[0], (other * K, 0), (K, F)),
-                lax.dynamic_slice(expert_up[0], (other * K, 0), (K, F)),
-            ],
-            axis=1,
-        )
-        if d > 0:
-            piece = lax.ppermute(piece, "tp", [(i, i ^ d) for i in range(T)])
-        both.append(piece)
 
     rot_query = rotate(
         query_rope.astype(f32).reshape(rows, heads, ROPE_DIM), places
@@ -350,41 +424,18 @@
         ],
         axis=2,
     ).reshape(rows, heads * LANES)
-    rope_in = jnp.zeros((width - rank, LANES), bf16)
-    rope_in = rope_in + jnp.asarray(
-        jnp.arange(width - rank)[:, None] + NOPE_DIM == jnp.arange(LANES)[None, :]
-    ).astype(bf16) * (jnp.arange(width - rank)[:, None] < ROPE_DIM).astype(bf16)
-    one_in = (
-        (jnp.arange(width - rank)[:, None] == ROPE_DIM)
-        & (jnp.arange(LANES)[None, :] == VALUE_DIM)
-    ).astype(bf16)
-
-    def widen(weight, size, tail):
+    spread = jnp.tile(
+        (jnp.arange(ROPE_DIM)[:, None] + NOPE_DIM == jnp.arange(LANES)[None, :]).astype(bf16),
+        (1, heads),
+    )
+
+    def widen(weight, size):
         weight = weight.reshape(rank, heads, size)
-        weight = jnp.pad(weight, ((0, 0), (0, 0), (0, LANES - size))).reshape(rank, heads * LANES)
-        return jnp.concatenate([weight, jnp.tile(tail, (1, heads))], axis=0)
-
-    wk = widen(key_up, NOPE_DIM, rope_in)
-    wv = widen(value_up, VALUE_DIM, one_in)
+        return jnp.pad(weight, ((0, 0), (0, 0), (0, LANES - size))).reshape(rank, heads * LANES)
+
+    wk = widen(key_up, NOPE_DIM)
+    wv = widen(value_up, VALUE_DIM)
     vmem = pl.BlockSpec(memory_space=pltpu.VMEM)
-    seq = S * rows
-    attended = pl.pallas_call(
-        functools.partial(attend_kernel, heads),
-        name="attend",
-        out_shape=jax.ShapeDtypeStruct((rows, heads * VALUE_DIM), bf16),
-        in_specs=[vmem] * 4,
-        out_specs=vmem,
-        scratch_shapes=[
-            pltpu.VMEM((heads, rows, LANES), f32),
-            pltpu.VMEM((heads, rows, LANES), f32),
-        ],
-        compiler_params=pltpu.CompilerParams(vmem_limit_bytes=48 * 2**20),
-        cost_estimate=pl.CostEstimate(
-            flops=4 * heads * rows * seq * LANES + 4 * seq * width * heads * LANES,
-            bytes_accessed=seq * width * 2,
-            transcendentals=heads * rows * seq,
-        ),
-    )(query, latents, wk, wv)
 
     experts = S * expert_gate.shape[0]
     capacity = 5 * rows * TOP_K // (4 * experts)
@@ -402,12 +453,17 @@
     anywhere = pl.BlockSpec(memory_space=pl.ANY)
     dma = pltpu.SemaphoreType.DMA
     return pl.pallas_call(
-        functools.partial(expert_kernel, S, T, C, M),
-        name="experts",
+        functools.partial(layer_kernel, S, T, C, M, heads),
+        name="layer",
         out_shape=jax.ShapeDtypeStruct((rows, K), bf16),
-        in_specs=[vmem] * 6 + [anywhere] * (T + 1),
+        in_specs=[vmem] * 9 + [anywhere] * 4,
         out_specs=vmem,
         scratch_shapes=[
+            pltpu.VMEM((S,) + packed.shape, bf16),
+            pltpu.VMEM((heads, rows, LANES), f32),
+            pltpu.VMEM((heads, rows, LANES), f32),
+            pltpu.VMEM((heads, rows, LANES), f32),
+            pltpu.VMEM((rows, heads * VALUE_DIM), bf16),
             pltpu.VMEM((T - 1, rows, heads * VALUE_DIM), bf16),
             pltpu.VMEM((8, rows), f32),
             pltpu.VMEM((T - 1, 8, rows), f32),
@@ -422,9 +478,12 @@
             pltpu.VMEM((S, T, C, F), bf16),
             pltpu.VMEM((S, C, K), bf16),
             pltpu.VMEM((S, C, K), bf16),
-            pltpu.VMEM((T, K, 2 * F), bf16),
+            pltpu.VMEM(out_proj.shape, bf16),
+            pltpu.VMEM((T, K, F), bf16),
+            pltpu.VMEM((T, K, F), bf16),
             pltpu.VMEM(expert_down.shape[1:], bf16),
-            dma((T + 1,)),
+            dma((4,)),
+            dma((S,)), dma((S,)), dma((S,)), dma((2, T - 1)), dma((2, T - 1)),
             dma((T - 1,)), dma((T - 1,)), dma((T - 1,)), dma((T - 1,)),
             dma((S,)), dma((S,)),
             dma((M, T - 1)), dma((M, T - 1)), dma((M, T - 1)), dma((M, T - 1)),
@@ -436,7 +495,10 @@
         cost_estimate=pl.CostEstimate(
             flops=6 * S * C * K * F * T, bytes_accessed=8 * K * K * 2, transcendentals=S * C * F
         ),
-    )(attended, residual, out_proj, norm_gain[None, :], slot_rows, slot_cols, *both, expert_down[0])
+    )(
+        query, packed, wk, wv, spread, residual, norm_gain[None, :], slot_rows, slot_cols,
+        out_proj, expert_gate[0], expert_up[0], expert_down[0],
+    )
 
 
 def solution(mesh):

time: 230 us -> 176 us (0.77)
  waiting for transfers between devices: 59.8 us -> 0 us
  Pallas kernels: 135 us -> 160 us
  between operations: 13.7 us -> 0.15 us
  starting transfers between devices: 2.65 us -> 0 us
    all_gather x1 -> x0, waiting for transfers between devices: 59.7 us -> none  [per_device(): latents = lax.all_gather(packed, ('sp', 'tp'), axis=0, tiled=True)]
    pallas_call x2 -> x1, Pallas kernels: 135 us -> 160 us  [per_device(): pl.pallas_call(functools.partial(layer_kernel, S, T, C, M, heads), name='...]
    concatenate x6 -> x1, other arithmetic: 4.42 us -> 0.79 us  [per_device(): jnp.concatenate([norm_rows(latent, latent_gain), folded.reshape(rows // f...]
    ppermute x3 -> x0, starting transfers between devices: 2.65 us -> none  [per_device(): piece = lax.ppermute(piece, 'tp', [(i, i ^ d) for i in range(T)])]
    dynamic_slice x2 -> x0, local copies, waits for them, and re-layouts: 2.52 us -> none  [the longest x1 2.43 us: per_device(): lax.dynamic_slice(expert_up[0], (other * K, 0), (K, F))]
    unnamed x28 -> x18, local copies, waits for them, and re-layouts: 5.75 us -> 4.15 us
  transfers between devices with their start and end apart: 4 -> 0, of which waited for: 1 -> 0; matrix products, arithmetic and copies ran while one was open for 4% -> 0% of each run, Pallas kernels for 5% -> 0%
where the time goes in v2:
time: 176 us; the launch traced here: 175 us
  Pallas kernels  160 us (91%)
  local copies, waits for them, and re-layouts  8.82 us (5%)
  other arithmetic  6.29 us (4%)
    pallas_call x1, Pallas kernels, per_device(): pl.pallas_call(functools.partial(layer_kernel, S, T, C, M, heads), name='...  160 us
    unnamed x18, local copies, waits for them, and re-layouts  4.15 us

profile of v2, /device:TPU:9, one launch (start us, length us, event | category | flops | bytes accessed | tf_op | source)
XLA Modules:
  0.0 175.1 jit_solution(5927963574715806187)
XLA Ops:
  0.1 1.2 fusion
  1.3 0.7 convert_reduce_fusion
  2.0 0.1 fusion.3
  2.1 0.8 select_reduce_fusion
  2.9 0.7 multiply_add_fusion
  3.6 0.7 pad_maximum_fusion.1
  4.4 0.6 copy.68
  5.0 0.7 convert_element_type.44
  5.8 0.2 subtract_convert_fusion.1
  6.1 0.2 copy.56
  6.3 0.2 copy.57
  6.6 0.1 reshape.135
  6.8 1.0 copy.54
  7.8 0.8 copy.62.cols_ref
  8.7 0.2 copy.53
  9.0 0.9 copy.63.q_ref
  9.9 0.1 copy.58
  10.1 1.0 copy.64.wk_ref
  11.2 0.1 copy.60
  11.3 1.0 copy.65.wv_ref
  12.4 0.2 fusion.2
  12.5 0.8 pad_maximum_fusion.lat_ref
  13.3 159.7 %layer.1 = bf16[384,1024]{1,0:T(8,128)(2,1)} custom-call(bf16[384,512]{1,0:T(8,128)(2,1)} %copy.63.q_ref, bf16[408,512]{1,0:T(8,128)(2,1)} %pad_maximum_fusion.lat_ref, bf16[512,512]{1,0:T(8,128)(2,1)} %copy.64.wk_ref, bf16[512,512]{1,0:T(8,128)(2,1)} %copy.65.wv_ref, bf16[32,512]{1,0:T(8,128)(2,1)} %bitcast.32, bf16[384,1024]{1,0:T(8,128)(2,1)} %res_ref.1, ...), custom_call_target="tpu_custom_call" | custom-call | flops 6039797760 | bytes 16777216 | tf_op jit(solution)/shard_map/layer/pallas_call | solution.py:455
  173.1 2.1 %copy.70 = bf16[384,1024]{1,0:T(8,128)(2,1)} copy(bf16[384,1024]{1,0:T(8,128)(2,1)} %layer.1) | data formatting | bytes 1572864
  (28 shorter events, 0.8 us)
Async XLA Ops:
  0.0 8.7 %copy-start.3 = (bf16[384,256]{1,0:T(8,128)(2,1)S(1)}, bf16[384,256]{1,0:T(8,128)(2,1)}, u32[]{:S(2)}) copy-start(bf16[384,256]{1,0:T(8,128)(2,1)} %param.16) | copy-start | bytes 589828
  2.1 7.8 %copy-start.1 = (bf16[512,256]{1,0:T(8,128)(2,1)S(1)}, bf16[512,256]{1,0:T(8,128)(2,1)}, u32[]{:S(2)}) copy-start(bf16[512,256]{1,0:T(8,128)(2,1)} %param.21) | copy-start | bytes 786436
  3.6 6.5 %copy-start.4 = (f32[384,2]{0,1:T(2,128)}, f32[384,2]{0,1:T(2,128)S(1)}, u32[]{:S(2)}) copy-start(f32[384,2]{0,1:T(2,128)S(1)} %multiply_add_fusion) | copy-start | bytes 9220
  8.7 2.5 %copy-start.2 = (bf16[512,256]{1,0:T(8,128)(2,1)S(1)}, bf16[512,256]{1,0:T(8,128)(2,1)}, u32[]{:S(2)}) copy-start(bf16[512,256]{1,0:T(8,128)(2,1)} %param.22) | copy-start | bytes 786436
  10.1 2.3 %copy-start = (bf16[384,512]{1,0:T(8,128)(2,1)S(1)}, bf16[384,512]{1,0:T(8,128)(2,1)}, u32[]{:S(2)}) copy-start(bf16[384,512]{1,0:T(8,128)(2,1)} %param.18) | copy-start | bytes 1179652
  10.1 2.3 %copy-start.5 = (f32[512]{0:T(512)S(1)}, f32[512]{0:T(512)}, u32[]{:S(2)}) copy-start(f32[512]{0:T(512)} %param.20) | copy-start | bytes 6148

commit v3 on v2

--- a/solution.py
+++ b/solution.py
@@ -19,30 +19,6 @@
 MESH = pl.DeviceIdType.MESH
 bf16 = jnp.bfloat16
 f32 = jnp.float32
-
-
-def rotate(values_in, places):
-    half_dim = values_in.shape[-1] // 2
-    inverse = rope_base ** (-jnp.arange(half_dim, dtype=jnp.float32) / half_dim)
-    angles = places.astype(jnp.float32)[:, None] * inverse[None, :]
-    angles = angles.reshape((angles.shape[0],) + (1,) * (values_in.ndim - 2) + (half_dim,))
-    cosine = jnp.cos(angles)
-    sine_wave = jnp.sin(angles)
-    first_half = values_in[..., :half_dim]
-    second_half = values_in[..., half_dim:]
-    return jnp.concatenate(
-        [
-            first_half * cosine - second_half * sine_wave,
-            first_half * sine_wave + second_half * cosine,
-        ],
-        axis=-1,
-    )
-
-
-def norm_rows(values_in, gain_vec):
-    wide = values_in.astype(jnp.float32)
-    mean_square = jnp.mean(wide * wide, axis=-1, keepdims=True)
-    return (wide * lax.rsqrt(mean_square + epsilon) * gain_vec[None, :]).astype(jnp.bfloat16)
 
 
 def flip(a, b, n):
@@ -56,10 +32,10 @@
 
 def layer_kernel(
     S, T, C, M, heads,
-    q_ref, lat_ref, wk_ref, wv_ref, spread_ref, res_ref, gain_ref, slot_ref, cols_ref,
+    nope_ref, turn_ref, cos_ref, sin_ref, latent_ref, lat_gain_ref, ku_ref, vu_ref, res_ref, gain_ref, slot_ref, cols_ref,
     wo_hbm, gate_hbm, up_hbm, down_hbm,
     out_ref,
-    lat_all, top_ref, sum_ref, nume_ref, att_ref,
+    q_ref, lat_ref, wk_ref, wv_ref, lat_all, top_ref, sum_ref, nume_ref, att_ref,
     att_all, sq_own, sq_all, mid_ref, acc_ref, norm_ref, send, recv, psend, precv, own, hid, res, ret,
     wo_ref, gate_ref, up_ref, down_ref,
     load_sem, z_s, c_s, l_r, w_s, w_r,
@@ -87,6 +63,25 @@
     for load in loads:
         load.start()
 
+    wide = latent_ref[...].astype(f32)
+    mean_square = jnp.mean(wide * wide, axis=1, keepdims=True)
+    lat_ref[:rows, :] = (wide * lax.rsqrt(mean_square + epsilon) * lat_gain_ref[...]).astype(bf16)
+    rank = latent_ref.shape[1]
+    folds = rank // ROPE_DIM
+    fold_rows = rows // folds
+    width = turn_ref.shape[1]
+    swap = lax.broadcasted_iota(jnp.int32, (width, width), 0) == (
+        lax.broadcasted_iota(jnp.int32, (width, width), 1) ^ (ROPE_DIM // 2)
+    )
+    partner = jnp.dot(
+        turn_ref[...], jnp.where(swap, 1.0, 0.0).astype(bf16), preferred_element_type=f32
+    )
+    turned = turn_ref[...].astype(f32) * cos_ref[...] + partner * sin_ref[...]
+    key_turned = turned[:, heads * ROPE_DIM : (heads + 1) * ROPE_DIM]
+    lat_ref[rows:, :] = jnp.concatenate(
+        [key_turned[q * fold_rows : (q + 1) * fold_rows, :] for q in range(folds)], axis=1
+    ).astype(bf16)
+
     barrier = pltpu.get_barrier_semaphore()
     for d in range(1, T):
         pl.semaphore_signal(barrier, inc=1, device_id=(me_s, flip(me_t, d, T)), device_id_type=MESH)
@@ -158,14 +153,42 @@
 
     for d in range(1, T):
         gate_copy(d).start()
-        up_copy(d).start()
+
+    def spaced(parts):
+        return jnp.concatenate(parts, axis=1).astype(bf16)
+
+    for h in range(heads):
+        cols = slice(h * LANES, (h + 1) * LANES)
+        q_ref[:, cols] = spaced(
+            [
+                nope_ref[:, h * NOPE_DIM : (h + 1) * NOPE_DIM].astype(f32),
+                turned[:, h * ROPE_DIM : (h + 1) * ROPE_DIM],
+                jnp.zeros((rows, LANES - NOPE_DIM - ROPE_DIM), f32),
+            ]
+        )
+        wk_ref[:, cols] = spaced(
+            [
+                ku_ref[:, h * NOPE_DIM : (h + 1) * NOPE_DIM].astype(f32),
+                jnp.zeros((rank, LANES - NOPE_DIM), f32),
+            ]
+        )
+        wv_ref[:, cols] = spaced(
+            [
+                vu_ref[:, h * VALUE_DIM : (h + 1) * VALUE_DIM].astype(f32),
+                jnp.zeros((rank, LANES - VALUE_DIM), f32),
+            ]
+        )
+    spread = jnp.where(
+        lax.broadcasted_iota(jnp.int32, (ROPE_DIM, heads * LANES), 0) + NOPE_DIM
+        == lax.broadcasted_iota(jnp.int32, (ROPE_DIM, heads * LANES), 1) % LANES,
+        1.0,
+        0.0,
+    ).astype(bf16)
 
     scale = (NOPE_DIM + ROPE_DIM) ** (-0.5) * 1.4426950408889634
     top_ref[...] = jnp.full(top_ref.shape, negative, f32)
     nume_ref[...] = jnp.zeros(nume_ref.shape, f32)
     sum_ref[...] = jnp.zeros(sum_ref.shape, f32)
-    rank = lat_ref.shape[1]
-    folds = rank // ROPE_DIM
 
     def attend(block, masked):
         lat = block[:rows, :]
@@ -175,7 +198,7 @@
         ).astype(bf16)
         keys = (
             jnp.dot(lat, wk_ref[...], preferred_element_type=f32)
-            + jnp.dot(rope, spread_ref[...], preferred_element_type=f32)
+            + jnp.dot(rope, spread, preferred_element_type=f32)
         ).astype(bf16)
         values = jnp.dot(lat, wv_ref[...], preferred_element_type=f32).astype(bf16)
         for h in range(heads):
@@ -226,6 +249,8 @@
     att_ref[...] = jnp.concatenate(outs, axis=1).astype(bf16)
     for d in range(1, T):
         att_copy(d).start()
+    for d in range(1, T):
+        up_copy(d).start()
     loads[0].wait()
 
     def project(att, d):
@@ -405,36 +430,18 @@
     rank = latent.shape[1]
     F = expert_gate.shape[2]
 
+    width = -(-(heads + 1) * ROPE_DIM // LANES) * LANES
+    half = ROPE_DIM // 2
     places = me_s * rows + jnp.arange(rows, dtype=jnp.int32)
-    folds = rank // ROPE_DIM
-    rot_key = rotate(key_rope.astype(f32), places).astype(bf16)
-    folded = jnp.swapaxes(rot_key.reshape(folds, rows // folds, ROPE_DIM), 0, 1)
-    packed = jnp.concatenate(
-        [norm_rows(latent, latent_gain), folded.reshape(rows // folds, rank)], axis=0
+    lane = jnp.arange(width, dtype=jnp.int32)
+    inverse = rope_base ** (-(lane % half).astype(f32) / half)
+    angles = places.astype(f32)[:, None] * inverse[None, :]
+    cosine = jnp.cos(angles)
+    sine = jnp.where((lane % ROPE_DIM < half)[None, :], -jnp.sin(angles), jnp.sin(angles))
+    turn = jnp.concatenate(
+        [query_rope, key_rope, jnp.zeros((rows, width - (heads + 1) * ROPE_DIM), bf16)], axis=1
     )
-
-    rot_query = rotate(
-        query_rope.astype(f32).reshape(rows, heads, ROPE_DIM), places
-    ).astype(bf16)
-    query = jnp.concatenate(
-        [
-            query_nope.reshape(rows, heads, NOPE_DIM),
-            rot_query,
-            jnp.zeros((rows, heads, LANES - NOPE_DIM - ROPE_DIM), bf16),
-        ],
-        axis=2,
-    ).reshape(rows, heads * LANES)
-    spread = jnp.tile(
-        (jnp.arange(ROPE_DIM)[:, None] + NOPE_DIM == jnp.arange(LANES)[None, :]).astype(bf16),
-        (1, heads),
-    )
-
-    def widen(weight, size):
-        weight = weight.reshape(rank, heads, size)
-        return jnp.pad(weight, ((0, 0), (0, 0), (0, LANES - size))).reshape(rank, heads * LANES)
-
-    wk = widen(key_up, NOPE_DIM)
-    wv = widen(value_up, VALUE_DIM)
+    pack_shape = (rows + rows * ROPE_DIM // rank, rank)
     vmem = pl.BlockSpec(memory_space=pltpu.VMEM)
 
     experts = S * expert_gate.shape[0]
@@ -456,10 +463,14 @@
         functools.partial(layer_kernel, S, T, C, M, heads),
         name="layer",
         out_shape=jax.ShapeDtypeStruct((rows, K), bf16),
-        in_specs=[vmem] * 9 + [anywhere] * 4,
+        in_specs=[vmem] * 12 + [anywhere] * 4,
         out_specs=vmem,
         scratch_shapes=[
-            pltpu.VMEM((S,) + packed.shape, bf16),
+            pltpu.VMEM((rows, heads * LANES), bf16),
+            pltpu.VMEM(pack_shape, bf16),
+            pltpu.VMEM((rank, heads * LANES), bf16),
+            pltpu.VMEM((rank, heads * LANES), bf16),
+            pltpu.VMEM((S,) + pack_shape, bf16),
             pltpu.VMEM((heads, rows, LANES), f32),
             pltpu.VMEM((heads, rows, LANES), f32),
             pltpu.VMEM((heads, rows, LANES), f32),
@@ -496,7 +507,7 @@
             flops=6 * S * C * K * F * T, bytes_accessed=8 * K * K * 2, transcendentals=S * C * F
         ),
     )(
-        query, packed, wk, wv, spread, residual, norm_gain[None, :], slot_rows, slot_cols,
+        query_nope, turn, cosine, sine, latent, latent_gain[None, :], key_up, value_up, residual, norm_gain[None, :], slot_rows, slot_cols,
         out_proj, expert_gate[0], expert_up[0], expert_down[0],
     )
 

time: 176 us -> 177 us (level)
  Pallas kernels: 160 us -> 165 us
  local copies, waits for them, and re-layouts: 8.82 us -> 3.84 us
    pallas_call x1, Pallas kernels: 160 us -> 165 us  [per_device(): pl.pallas_call(functools.partial(layer_kernel, S, T, C, M, heads), name='...]
    reshape x4 -> x0, local copies, waits for them, and re-layouts: 3.09 us -> none  [the longest x2 2.01 us: widen(): jnp.pad(weight, ((0, 0), (0, 0), (0, LANES - size)))]
    select_n x0 -> x1, other arithmetic: none -> 2.49 us  [per_device(): jnp.where((lane % ROPE_DIM < half)[None, :], -jnp.sin(angles), jnp.sin(an...]
    unnamed x18 -> x4, local copies, waits for them, and re-layouts: 4.15 us -> 2.92 us
where the time goes in v3:
time: 177 us; the launch traced here: 176 us
  Pallas kernels  165 us (93%)
  other arithmetic  6.97 us (4%)
  local copies, waits for them, and re-layouts  3.84 us (2%)
    pallas_call x1, Pallas kernels, per_device(): pl.pallas_call(functools.partial(layer_kernel, S, T, C, M, heads), name='...  165 us

profile of v3, /device:TPU:9, one launch (start us, length us, event | category | flops | bytes accessed | tf_op | source)
XLA Modules:
  0.0 176.2 jit_solution(9070150806832727087)
XLA Ops:
  0.0 0.1 pad.4.clone
  0.1 0.7 convert_reduce_fusion
  0.8 0.1 fusion
  0.9 0.8 select_reduce_fusion
  1.7 0.7 multiply_add_fusion
  2.4 0.0 copy-start
  2.4 0.7 pad_maximum_fusion
  3.1 0.9 copy.27
  3.9 1.6 maximum_maximum_fusion.turn_ref
  5.6 0.8 copy.28.cols_ref
  6.4 2.5 %negate_select_fusion = (f32[384,256]{1,0:T(8,128)}, f32[384,256]{1,0:T(8,128)}) fusion(f32[256]{0:T(256)S(1)} %fusion.5, f32[384]{0:T(512)S(1)} %add_convert_fusion, pred[256]{0:T(512)(128)(4,1)S(1)} %fusion.6), kind=kLoop, calls=%fused_computation | loop fusion | flops 294912 | bytes 789248 | tf_op jit(solution)/shard_map/jit(_where)/select_n | solution.py:440
  8.9 0.0 copy-done
  8.9 165.2 %layer.1 = bf16[384,1024]{1,0:T(8,128)(2,1)} custom-call(bf16[384,256]{1,0:T(8,128)(2,1)} %nope_ref.1, bf16[384,256]{1,0:T(8,128)(2,1)} %maximum_maximum_fusion.turn_ref, f32[384,256]{1,0:T(8,128)} %get-tuple-element.6.cos_ref, f32[384,256]{1,0:T(8,128)} %get-tuple-element.5.sin_ref, bf16[384,512]{1,0:T(8,128)(2,1)} %latent_ref.1, f32[1,512]{1,0:T(1,128)} %bitcast.12, ...), custom_call_target="tpu_custom_call" | custom-call | flops 6039797760 | bytes 16777216 | tf_op jit(solution)/shard_map/layer/pallas_call | solution.py:462
  174.1 2.1 %copy.30 = bf16[384,1024]{1,0:T(8,128)(2,1)} copy(bf16[384,1024]{1,0:T(8,128)(2,1)} %layer.1) | data formatting | bytes 1572864
  (4 shorter events, 0.0 us)
Async XLA Ops:
  2.4 6.5 %copy-start = (f32[384,2]{0,1:T(2,128)}, f32[384,2]{0,1:T(2,128)S(1)}, u32[]{:S(2)}) copy-start(f32[384,2]{0,1:T(2,128)S(1)} %multiply_add_fusion) | copy-start | bytes 9220
